TPU v7x, 256 devices: a whole 4x4x8 slice. The times are simulated.
256 devices in a mesh: sp: 32 (over z, x), tp: 8 (over y, core).
Axes of the slice: x: 4, y: 4, z: 8, core: 2. Of those that a mesh axis runs over, the one named last changes fastest.
Arguments:
- features: bfloat16 [12288, 2048], P('sp', 'tp'), may hold values from -6 to 6
- norm_gain: float32 [2048], replicated, may hold values from 0.28 to 10
- w_query: bfloat16 [2048, 1024], P(None, 'tp'), may hold values from -0.125 to 0.125
- w_key: bfloat16 [2048, 512], P(None, 'tp'), may hold values from -0.125 to 0.125
- w_value: bfloat16 [2048, 512], P(None, 'tp'), may hold values from -0.125 to 0.125
- head_sinks: float32 [16], P('tp'), may hold values from 1 to 5
- w_query_latent: bfloat16 [2048, 512], replicated, may hold values from -0.125 to 0.125
- w_kv_latent: bfloat16 [2048, 512], replicated, may hold values from -0.125 to 0.125
- w_rope_key: bfloat16 [2048, 64], replicated, may hold values from -0.125 to 0.125
- query_latent_gain: float32 [512], replicated, may hold values from 0.28 to 10
- kv_latent_gain: float32 [512], replicated, may hold values from 0.28 to 10
- w_query_content: bfloat16 [512, 1024], P(None, 'tp'), may hold values from -0.25 to 0.25
- w_query_rotary: bfloat16 [512, 512], P(None, 'tp'), may hold values from -0.25 to 0.25
- w_key_up: bfloat16 [512, 1024], P(None, 'tp'), may hold values from -0.25 to 0.25
- w_value_up: bfloat16 [512, 1024], P(None, 'tp'), may hold values from -0.25 to 0.25
- w_branch_window: bfloat16 [1024, 2048], P('tp'), may hold values from -0.1875 to 0.1875
- w_branch_latent: bfloat16 [1024, 2048], P('tp'), may hold values from -0.1875 to 0.1875
- w_gate_window: bfloat16 [2048, 2048], P(None, 'tp'), may hold values from -0.125 to 0.125
- w_gate_latent: bfloat16 [2048, 2048], P(None, 'tp'), may hold values from -0.125 to 0.125
Outputs:
- mixed: bfloat16 [12288, 2048], P('sp', 'tp')
All inputs are finite; a program needn't handle non-finite values.
Results may differ from a plain program's by a relative error of at most 0.018.
The roundings to bfloat16 on the way count: a program that leaves them out, or rounds other values in their place, can miss the bound.
Values may be sent and summed in bfloat16 or wider, within the bound.
A program may use at most 128 MiB of HBM per device.

v0:
```python
import jax
import jax.numpy as jnp
from jax import lax
from jax.sharding import PartitionSpec as P

HEAD = 64
WINDOW = 128
NOPE = 128
ROPE = 64
VDIM = 128
EPS = 1e-06
THETA = 10000.0
NEGATIVE = -1e30


def copy_for_each(shard, axis):
    count = lax.axis_size(axis)
    return lax.all_to_all(
        jnp.broadcast_to(shard[None], (count, *shard.shape)), axis, 0, 0, tiled=True
    )


def in_order(parts, dim):
    shape = list(parts.shape[1:])
    shape[dim] *= parts.shape[0]
    return jnp.moveaxis(parts, 0, dim).reshape(shape)


def gathered_copies(shard, axis, dim):
    parts = copy_for_each(shard, axis)
    return in_order(parts, dim)


def from_behind(shard, axis, by):
    count = lax.axis_size(axis)
    pairs = [(i, i + by) for i in range(count) if 0 <= i + by < count]
    return lax.ppermute(shard, axis, pairs)


def in_one_piece(arrays, axis, dim, along):
    widths = [a.shape[along] for a in arrays]
    both = jnp.concatenate(arrays, axis=along)
    result = lax.all_gather(both, axis, axis=dim, tiled=True)
    return tuple(jnp.split(result, [sum(widths[:k]) for k in range(1, len(widths))], axis=along))


def rms_rows(float_rows, gain_vec):
    return (
        float_rows
        * lax.rsqrt(jnp.mean(float_rows * float_rows, axis=-1, keepdims=True) + EPS)
        * gain_vec
    )


def rotate(float_rows, positions):
    half_width = float_rows.shape[-1] // 2
    frequencies = THETA ** (-jnp.arange(half_width, dtype=jnp.float32) / half_width)
    angles = positions.astype(jnp.float32)[:, None] * frequencies
    target = (float_rows.shape[0],) + (1,) * (float_rows.ndim - 2) + (half_width,)
    cosine = jnp.cos(angles).reshape(target)
    sine_part = jnp.sin(angles).reshape(target)
    first_half = float_rows[..., :half_width]
    second_half = float_rows[..., half_width:]
    return jnp.concatenate(
        [
            first_half * cosine - second_half * sine_part,
            second_half * cosine + first_half * sine_part,
        ],
        axis=-1,
    )


def project(left, right):
    return jnp.dot(left, right, preferred_element_type=jnp.float32)


def window_attention(queries, key_ext, value_ext, sink_table, row_start):
    row_count = queries.shape[0]
    kv_heads = key_ext.shape[1] // HEAD
    group_size = queries.shape[1] // HEAD // kv_heads
    blocks = row_count // WINDOW
    query_blocks = queries.reshape(blocks, WINDOW, kv_heads, group_size, HEAD)

    def banded(table):
        table = table.reshape(blocks + 1, WINDOW, kv_heads, HEAD)
        return jnp.concatenate([table[:-1], table[1:]], axis=1)

    key_band = banded(key_ext)
    value_band = banded(value_ext)
    scores = jnp.einsum(
        "nqhgd,nkhd->nhgqk", query_blocks, key_band, preferred_element_type=jnp.float32
    ) * HEAD ** (-0.5)
    query_index = jnp.arange(WINDOW, dtype=jnp.int32)[:, None]
    key_index = jnp.arange(2 * WINDOW, dtype=jnp.int32)[None, :]
    offset = query_index + WINDOW - key_index
    key_position = (
        row_start + jnp.arange(blocks, dtype=jnp.int32)[:, None, None] * WINDOW + key_index - WINDOW
    )
    valid_mask = ((offset >= 0) & (offset < WINDOW) & (key_position >= 0))[:, None, None]
    scores = jnp.where(valid_mask, scores, NEGATIVE)
    sink_logit = sink_table.reshape(1, kv_heads, group_size, 1, 1)
    row_top = jnp.maximum(jnp.max(scores, axis=-1, keepdims=True), sink_logit)
    weights = jnp.where(valid_mask, jnp.exp(scores - row_top), 0.0)
    denominator = jnp.sum(weights, axis=-1, keepdims=True) + jnp.exp(sink_logit - row_top)
    probabilities = (weights / denominator).astype(jnp.bfloat16)
    attended = jnp.einsum(
        "nhgqk,nkhd->nqhgd", probabilities, value_band, preferred_element_type=jnp.float32
    )
    return attended.astype(jnp.bfloat16).reshape(row_count, kv_heads * group_size * HEAD)


def on_device(
    features,
    norm_gain,
    w_query,
    w_key,
    w_value,
    head_sinks,
    w_query_latent,
    w_kv_latent,
    w_rope_key,
    query_latent_gain,
    kv_latent_gain,
    w_query_content,
    w_query_rotary,
    w_key_up,
    w_value_up,
    w_branch_window,
    w_branch_latent,
    w_gate_window,
    w_gate_latent,
):
    tok_rows = features.shape[0]
    row_start = lax.axis_index("sp") * tok_rows
    row_end = row_start + tok_rows
    positions = row_start + jnp.arange(tok_rows, dtype=jnp.int32)
    gathered = gathered_copies(features, "tp", 1)
    normed = rms_rows(gathered.astype(jnp.float32), norm_gain).astype(jnp.bfloat16)
    query_rows = project(normed, w_query).astype(jnp.bfloat16)
    key_rows = project(normed, w_key).astype(jnp.bfloat16)
    value_rows = project(normed, w_value).astype(jnp.bfloat16)
    key_width = key_rows.shape[1]
    packed = jnp.concatenate([key_rows, value_rows], axis=1)
    tail_rows = from_behind(packed[tok_rows - WINDOW :], "sp", 1)
    extended = jnp.concatenate([tail_rows, packed], axis=0)
    window_out = window_attention(
        query_rows, extended[:, :key_width], extended[:, key_width:], head_sinks, row_start
    )
    latent_query = rms_rows(project(normed, w_query_latent), query_latent_gain).astype(jnp.bfloat16)
    latent_kv = rms_rows(project(normed, w_kv_latent), kv_latent_gain).astype(jnp.bfloat16)
    rope_rows = rotate(project(normed, w_rope_key), positions).astype(jnp.bfloat16)
    lat_heads = w_key_up.shape[1] // NOPE
    query_content = (
        project(latent_query, w_query_content)
        .astype(jnp.bfloat16)
        .reshape(tok_rows, lat_heads, NOPE)
    )
    query_rotary = rotate(
        project(latent_query, w_query_rotary).reshape(tok_rows, lat_heads, ROPE), positions
    ).astype(jnp.bfloat16)
    scale_factor = (NOPE + ROPE) ** (-0.5)

    def attend(running, piece_keys, piece_values, rope_piece):
        running_max, denominator, accumulated = running
        piece_rows = piece_keys.shape[0]
        scores = (
            jnp.einsum(
                "qhd,khd->hqk",
                query_content,
                piece_keys.reshape(piece_rows, lat_heads, NOPE),
                preferred_element_type=jnp.float32,
            )
            + jnp.einsum(
                "qhr,kr->hqk", query_rotary, rope_piece, preferred_element_type=jnp.float32
            )
        ) * scale_factor
        key_position = jnp.arange(piece_rows, dtype=jnp.int32)
        live_mask = key_position[None, :] <= positions[:, None]
        scores = jnp.where(live_mask, scores, NEGATIVE)
        new_max = jnp.maximum(running_max, jnp.max(scores, axis=-1))
        weights = jnp.where(live_mask, jnp.exp(scores - new_max[..., None]), 0.0)
        denominator = jnp.sum(weights, axis=-1)
        accumulated = jnp.einsum(
            "hqk,khd->hqd",
            weights.astype(jnp.bfloat16),
            piece_values.reshape(piece_rows, lat_heads, VDIM),
            preferred_element_type=jnp.float32,
        )
        return (new_max, denominator, accumulated)

    initial = (
        jnp.full((lat_heads, tok_rows), NEGATIVE, jnp.float32),
        jnp.zeros((lat_heads, tok_rows), jnp.float32),
        jnp.zeros((lat_heads, tok_rows, VDIM), jnp.float32),
    )
    own_keys = project(latent_kv, w_key_up).astype(jnp.bfloat16)
    own_values = project(latent_kv, w_value_up).astype(jnp.bfloat16)
    pieces = in_one_piece((own_keys, own_values, rope_rows), "sp", 0, 1)
    running = lax.cond(
        jnp.int32(0) < row_end,
        lambda current: attend(current, pieces[0], pieces[1], pieces[2]),
        lambda current: current,
        initial,
    )
    latent_out = jnp.transpose(running[2] / running[1][..., None], (1, 0, 2))
    latent_out = latent_out.reshape(tok_rows, lat_heads * VDIM).astype(jnp.bfloat16)
    all_window, all_latent = in_one_piece((window_out, latent_out), "tp", 1, 0)
    column_window, column_latent = (
        lax.all_to_all(w_branch_window, "tp", split_axis=1, concat_axis=0, tiled=True),
        lax.all_to_all(w_branch_latent, "tp", split_axis=1, concat_axis=0, tiled=True),
    )
    window_branch = project(all_window, column_window)
    latent_branch = project(all_latent, column_latent)
    window_gate = jax.nn.sigmoid(project(normed, w_gate_window))
    latent_gate = jax.nn.sigmoid(project(normed, w_gate_latent))
    return (window_gate * window_branch + latent_gate * latent_branch).astype(jnp.bfloat16)


def solution(mesh):
    return jax.shard_map(
        on_device,
        mesh=mesh,
        in_specs=(
            P("sp", "tp"),
            P(),
            P(None, "tp"),
            P(None, "tp"),
            P(None, "tp"),
            P("tp"),
            P(),
            P(),
            P(),
            P(),
            P(),
            P(None, "tp"),
            P(None, "tp"),
            P(None, "tp"),
            P(None, "tp"),
            P("tp", None),
            P("tp", None),
            P(None, "tp"),
            P(None, "tp"),
        ),
        out_specs=P("sp", "tp"),
        check_vma=False,
    )
```

profile of v0, /device:TPU:36, one launch (start us, length us, event | category | flops | bytes accessed | tf_op | source)
XLA Modules:
  0.0 250.7 jit_solution(12856816892344930347)
XLA Ops:
  6.5 1.2 copy.42
  7.8 1.3 broadcast_in_dim.36
  9.1 4.5 %all-to-all-start = ((bf16[8,384,256]{1,2,0:T(8,128)(2,1)}), bf16[8,384,256]{1,2,0:T(8,128)(2,1)}, u32[]{:S(2)}, u32[]{:S(2)}) async-start(bf16[8,384,256]{1,2,0:T(8,128)(2,1)} %broadcast_in_dim.36), calls=%async_computation | async-start | bytes 3145728 | tf_op jit(solution)/shard_map/all_to_all | solution.py:18
  13.6 21.6 %all-to-all-done = bf16[8,384,256]{1,2,0:T(8,128)(2,1)} async-done(((bf16[8,384,256]{1,2,0:T(8,128)(2,1)}), bf16[8,384,256]{1,2,0:T(8,128)(2,1)}, u32[]{:S(2)}, u32[]{:S(2)}) %all-to-all-start) | async-done | bytes 1572896 | tf_op jit(solution)/shard_map/all_to_all | solution.py:18
  35.2 1.8 multiply_reduce_fusion
  37.0 1.8 fusion.19
  38.9 1.1 multiply_reduce_fusion.2
  41.5 0.7 pad_maximum_fusion
  42.6 1.9 convolution_convert_fusion.5
  44.6 1.8 convolution_convert_fusion.6
  46.4 3.2 %collective-permute-start = (bf16[128,128]{0,1:T(8,128)(2,1)S(1)}, bf16[128,128]{0,1:T(8,128)(2,1)S(1)}, u32[]{:S(2)}, u32[]{:S(2)}) collective-permute-start(bf16[128,128]{0,1:T(8,128)(2,1)S(1)} %pad_maximum_fusion.6), channel_id=1, source_target_pairs={{0,8},{8,16},{16,24},{24,32},{32,40},{40,48},{48,56},{56,64},{64,7... | collective-permute-start | bytes 98312 | tf_op jit(solution)/shard_map/ppermute | solution.py:37
  49.7 1.1 multiply_reduce_fusion.1
  51.8 0.6 convolution_convert_fusion.4
  53.8 89.5 %all-gather.3.cloned.1.call-done = bf16[12288,320]{0,1:T(8,128)(2,1)} async-done(((bf16[384,320]{0,1:T(8,128)(2,1)}), bf16[12288,320]{0,1:T(8,128)(2,1)}) %all-gather.3.cloned.1.call-update) | async-done | bytes 7864336 | tf_op jit(solution)/shard_map/all_gather | solution.py:43
  143.3 59.5 %conditional.1 = (f32[1,384]{1,0:T(1,128)S(1)}, f32[1,384,128]{1,2,0:T(8,128)S(1)}) conditional(s32[]{:T(128)} %convert_element_type.97, () %tuple.13, (s32[]{:T(128)}, s32[384]{0:T(512)S(1)}, bf16[12288,320]{0,1:T(8,128)(2,1)}, bf16[384,128]{1,0:T(8,128)(2,1)S(1)}, bf16[384,1,64]{0,2,1:T(8,128)(2,1)S(1)}) %tuple.14), branch_computations={%region_5.6_spmd, %region_6.9_spmd} | conditional | flops 3081240576 | bytes 119901712 | solution.py:199
  143.3 11.6 %copy.51 = bf16[12288,320]{1,0:T(8,128)(2,1)} copy(bf16[12288,320]{0,1:T(8,128)(2,1)} %get-tuple-element.44) | data formatting | bytes 15728640 | tf_op jit(solution)/shard_map
  154.9 9.8 %fusion.9 = f32[384,12288]{1,0:T(8,128)} fusion(bf16[384,128]{1,0:T(8,128)(2,1)S(1)} %get-tuple-element.25, bf16[12288,320]{1,0:T(8,128)(2,1)} %copy.51), kind=kOutput, calls=%fused_computation.11 | convolution fusion | flops 1207959552 | bytes 22118400 | tf_op jit(solution)/shard_map/cond/branch_1_fun/qhd,khd->hqk/dot_general | solution.py:167
  164.7 16.8 %fusion.63 = (f32[384]{0:T(512)S(1)}, f32[1,384,12288]{2,1,0:T(8,128)}) fusion(bf16[384,1,64]{0,2,1:T(8,128)(2,1)S(1)} %get-tuple-element.27, bf16[12288,320]{1,0:T(8,128)(2,1)} %copy.51, f32[384,12288]{1,0:T(8,128)} %fusion.9, s32[384]{0:T(512)S(1)} %broadcast_add_fusion), kind=kOutput, calls=%fused_computation.111 | convolution fusion | flops 627572352 | bytes 40946688 | tf_op jit(solution)/shard_map/cond/branch_1_fun/qhr,kr->hqk/dot_general | solution.py:173
  181.5 10.2 %fusion.11 = f32[1,384,128]{1,2,0:T(8,128)S(1)} fusion(bf16[12288,320]{1,0:T(8,128)(2,1)} %copy.51, f32[1,384,12288]{2,1,0:T(8,128)} %get-tuple-element.49, f32[384]{0:T(512)S(1)} %broadcast_maximum_fusion, s32[384]{0:T(512)S(1)} %broadcast_add_fusion), kind=kOutput, calls=%fused_computation.13 | convolution fusion | flops 1226833920 | bytes 22219776 | tf_op jit(solution)/shard_map/cond/branch_1_fun/hqk,khd->hqd/dot_general | solution.py:183
  191.7 11.1 %fusion.3 = f32[384]{0:T(512)S(1)} fusion(f32[1,384,12288]{2,1,0:T(8,128)} %get-tuple-element.49, f32[384]{0:T(512)S(1)} %broadcast_maximum_fusion, s32[384]{0:T(512)S(1)} %broadcast_add_fusion), kind=kLoop, calls=%fused_computation.6 | loop fusion | flops 18873984 | bytes 18878976 | tf_op jit(solution)/shard_map/cond/branch_1_fun/reduce_sum | solution.py:182
  202.9 0.7 pad_maximum_fusion.1
  203.6 1.0 copy.55
  204.6 4.3 %all-to-all-start.2 = ((bf16[128,8,256]{0,2,1:T(8,128)(2,1)}), bf16[128,8,256]{0,2,1:T(8,128)(2,1)S(1)}, u32[]{:S(2)}, u32[]{:S(2)}) async-start(bf16[128,8,256]{0,2,1:T(8,128)(2,1)} %bitcast.24), calls=%async_computation.2 | async-start | bytes 1048576 | tf_op jit(solution)/shard_map/all_to_all | solution.py:210
  208.9 1.0 copy.53
  209.9 10.4 %all-to-all-done.2 = bf16[128,8,256]{0,2,1:T(8,128)(2,1)S(1)} async-done(((bf16[128,8,256]{0,2,1:T(8,128)(2,1)}), bf16[128,8,256]{0,2,1:T(8,128)(2,1)S(1)}, u32[]{:S(2)}, u32[]{:S(2)}) %all-to-all-start.2) | async-done | bytes 524320 | tf_op jit(solution)/shard_map/all_to_all | solution.py:210
  220.3 3.7 %all-to-all-start.1 = ((bf16[128,8,256]{0,2,1:T(8,128)(2,1)}), bf16[128,8,256]{0,2,1:T(8,128)(2,1)S(1)}, u32[]{:S(2)}, u32[]{:S(2)}) async-start(bf16[128,8,256]{0,2,1:T(8,128)(2,1)} %bitcast.21), calls=%async_computation.1 | async-start | bytes 1048576 | tf_op jit(solution)/shard_map/all_to_all | solution.py:209
  224.2 9.8 %all-to-all-done.1 = bf16[128,8,256]{0,2,1:T(8,128)(2,1)S(1)} async-done(((bf16[128,8,256]{0,2,1:T(8,128)(2,1)}), bf16[128,8,256]{0,2,1:T(8,128)(2,1)S(1)}, u32[]{:S(2)}, u32[]{:S(2)}) %all-to-all-start.1) | async-done | bytes 524320 | tf_op jit(solution)/shard_map/all_to_all | solution.py:209
  234.0 1.0 copy.54
  235.1 2.7 %fusion.28 = f32[384,256]{1,0:T(8,128)} fusion(bf16[384,2048]{0,1:T(8,128)(2,1)S(1)} %copy-done.3, bf16[2048,256]{1,0:T(8,128)(2,1)} %param.39), kind=kOutput, calls=%fused_computation.35 | convolution fusion | flops 402948096 | bytes 3014656 | tf_op jit(solution)/shard_map/dot_general | solution.py:74
  237.8 2.2 fusion.25
  240.0 1.6 convolution_multiply_fusion.1
  241.6 2.2 fusion.29
  (91 shorter events, 4.5 us)
Async XLA Ops:
  6.5 32.3 %copy-start = (bf16[2048,512]{1,0:T(8,128)(2,1)S(1)}, bf16[2048,512]{1,0:T(8,128)(2,1)}, u32[]{:S(2)}) copy-start(bf16[2048,512]{1,0:T(8,128)(2,1)} %param.28) | copy-start | bytes 6291460
  7.8 29.2 %copy-start.15 = (f32[2048]{0:T(1024)S(1)}, f32[2048]{0:T(1024)}, u32[]{:S(2)}) copy-start(f32[2048]{0:T(1024)} %param.22) | copy-start | bytes 24580
  9.1 26.1 %all-to-all-start = ((bf16[8,384,256]{1,2,0:T(8,128)(2,1)}), bf16[8,384,256]{1,2,0:T(8,128)(2,1)}, u32[]{:S(2)}, u32[]{:S(2)}) async-start(bf16[8,384,256]{1,2,0:T(8,128)(2,1)} %broadcast_in_dim.36), calls=%async_computation | async-start | bytes 3145728 | tf_op jit(solution)/shard_map/all_to_all | solution.py:18
  13.5 129.8 %all-gather.3.cloned.1.call-start = ((), (), s32[]{:S(2)}) async-start(), calls=%async_computation.3 | async-start | bytes 8110080 | tf_op jit(solution)/shard_map/all_gather | solution.py:43
  38.9 2.0 copy-start.2
  38.9 1.2 copy-start.11
  38.9 1.2 copy-start.16
  38.9 1.5 copy-start.12
  38.9 1.9 copy-start.10
  40.0 2.6 %copy-start.8 = (bf16[2048,64]{0,1:T(8,128)(2,1)S(1)}, bf16[2048,64]{0,1:T(8,128)(2,1)}, u32[]{:S(2)}) copy-start(bf16[2048,64]{0,1:T(8,128)(2,1)} %param.25) | copy-start | bytes 786436
  40.4 4.1 %copy-start.9 = (bf16[2048,64]{0,1:T(8,128)(2,1)S(1)}, bf16[2048,64]{0,1:T(8,128)(2,1)}, u32[]{:S(2)}) copy-start(bf16[2048,64]{0,1:T(8,128)(2,1)} %param.24) | copy-start | bytes 786436
  41.2 8.4 %copy-start.3 = (bf16[384,2048]{0,1:T(8,128)(2,1)S(1)}, bf16[384,2048]{0,1:T(8,128)(2,1)}, u32[]{:S(2)}) copy-start(bf16[384,2048]{0,1:T(8,128)(2,1)} %copy-done.2) | copy-start | bytes 4718596
  42.3 197.7 %all-gather.5.cloned.1.call-start = ((), (), s32[]{:S(2)}) async-start(), calls=%async_computation.4 | async-start | bytes 1769472 | tf_op jit(solution)/shard_map/all_gather | solution.py:43
  42.3 7.4 %copy-start.19 = (bf16[2048,512]{1,0:T(8,128)(2,1)S(1)}, bf16[2048,512]{1,0:T(8,128)(2,1)}, u32[]{:S(2)}) copy-start(bf16[2048,512]{1,0:T(8,128)(2,1)} %param.27) | copy-start | bytes 6291460
  46.4 4.4 %copy-start.14 = (bf16[512,64]{0,1:T(8,128)(2,1)S(1)}, bf16[512,64]{0,1:T(8,128)(2,1)}, u32[]{:S(2)}) copy-start(bf16[512,64]{0,1:T(8,128)(2,1)} %param.33) | copy-start | bytes 196612
  46.4 4.4 %copy-start.17 = (f32[512]{0:T(512)S(1)}, f32[512]{0:T(512)}, u32[]{:S(2)}) copy-start(f32[512]{0:T(512)} %param.30) | copy-start | bytes 6148
  46.4 5.0 %copy-start.13 = (bf16[512,128]{1,0:T(8,128)(2,1)S(1)}, bf16[512,128]{1,0:T(8,128)(2,1)}, u32[]{:S(2)}) copy-start(bf16[512,128]{1,0:T(8,128)(2,1)} %param.32) | copy-start | bytes 393220
  46.4 5.4 %copy-start.7 = (bf16[2048,128]{1,0:T(8,128)(2,1)S(1)}, bf16[2048,128]{1,0:T(8,128)(2,1)}, u32[]{:S(2)}) copy-start(bf16[2048,128]{1,0:T(8,128)(2,1)} %param.23) | copy-start | bytes 1572868
  46.4 6.2 %collective-permute-start = (bf16[128,128]{0,1:T(8,128)(2,1)S(1)}, bf16[128,128]{0,1:T(8,128)(2,1)S(1)}, u32[]{:S(2)}, u32[]{:S(2)}) collective-permute-start(bf16[128,128]{0,1:T(8,128)(2,1)S(1)} %pad_maximum_fusion.6), channel_id=1, source_target_pairs={{0,8},{8,16},{16,24},{24,32},{32,40},{40,48},{48,56},{56,64},{64,7... | collective-permute-start | bytes 98312 | tf_op jit(solution)/shard_map/ppermute | solution.py:37
  51.4 1.6 copy-start.18
  143.3 60.3 %copy-start.4 = (bf16[128,2048]{1,0:T(8,128)(2,1)S(1)}, bf16[128,2048]{1,0:T(8,128)(2,1)}, u32[]{:S(2)}) copy-start(bf16[128,2048]{1,0:T(8,128)(2,1)} %param.37) | copy-start | bytes 1572868
  202.8 6.1 %copy-start.5 = (bf16[128,2048]{1,0:T(8,128)(2,1)S(1)}, bf16[128,2048]{1,0:T(8,128)(2,1)}, u32[]{:S(2)}) copy-start(bf16[128,2048]{1,0:T(8,128)(2,1)} %param.36) | copy-start | bytes 1572868
  204.6 15.7 %all-to-all-start.2 = ((bf16[128,8,256]{0,2,1:T(8,128)(2,1)}), bf16[128,8,256]{0,2,1:T(8,128)(2,1)S(1)}, u32[]{:S(2)}, u32[]{:S(2)}) async-start(bf16[128,8,256]{0,2,1:T(8,128)(2,1)} %bitcast.24), calls=%async_computation.2 | async-start | bytes 1048576 | tf_op jit(solution)/shard_map/all_to_all | solution.py:210
  220.3 13.7 %all-to-all-start.1 = ((bf16[128,8,256]{0,2,1:T(8,128)(2,1)}), bf16[128,8,256]{0,2,1:T(8,128)(2,1)S(1)}, u32[]{:S(2)}, u32[]{:S(2)}) async-start(bf16[128,8,256]{0,2,1:T(8,128)(2,1)} %bitcast.21), calls=%async_computation.1 | async-start | bytes 1048576 | tf_op jit(solution)/shard_map/all_to_all | solution.py:209
  235.1 2.7 %copy-start.20 = (bf16[2048,256]{1,0:T(8,128)(2,1)S(1)}, bf16[2048,256]{1,0:T(8,128)(2,1)}, u32[]{:S(2)}) copy-start(bf16[2048,256]{1,0:T(8,128)(2,1)} %param.38) | copy-start | bytes 3145732
  237.8 3.9 %copy-start.6 = (bf16[8,128,256]{2,1,0:T(8,128)(2,1)S(1)}, bf16[8,128,256]{2,1,0:T(8,128)(2,1)}, u32[]{:S(2)}) copy-start(bf16[8,128,256]{2,1,0:T(8,128)(2,1)} %copy.54) | copy-start | bytes 1572868
  237.8 6.1 %copy-start.1 = (bf16[2048,512]{1,0:T(8,128)(2,1)S(1)}, bf16[2048,512]{1,0:T(8,128)(2,1)}, u32[]{:S(2)}) copy-start(bf16[2048,512]{1,0:T(8,128)(2,1)} %param.28) | copy-start | bytes 6291460
Sparse Core Ops, SparseCore 0:
  42.4 100.8 all-gather.2
  203.7 27.3 all-gather.4
where the time goes:
time: 252 us; the launch traced here: 251 us
  waiting for transfers between devices  131 us (52%)
  matrix products  54.4 us (22%)
  local copies, waits for them, and re-layouts  17.9 us (7%)
  other arithmetic  17.4 us (7%)
  starting transfers between devices  15.8 us (6%)
  between operations  14 us (6%)
    all_gather x2, waiting for transfers between devices, in_one_piece(): result = lax.all_gather(both, axis, axis=dim, tiled=True)  89.5 us
    all_to_all x1, waiting for transfers between devices, copy_for_each(): lax.all_to_all(jnp.broadcast_to(shard[None], (count, *shard.shape)), axis...  21.6 us
    dot_general x14, matrix products, project(): return jnp.dot(left, right, preferred_element_type=jnp.float32)  17 us
    dot_general x1, matrix products, attend(): jnp.einsum('qhr,kr->hqk', query_rotary, rope_piece, preferred_element_typ...  16.8 us
    another operation x2, local copies, waits for them, and re-layouts  11.7 us
    reduce_sum x1, other arithmetic, attend(): denominator = jnp.sum(weights, axis=-1)  11.1 us
    all_to_all x1, waiting for transfers between devices, on_device(): lax.all_to_all(w_branch_latent, 'tp', split_axis=1, concat_axis=0, tiled=...  10.4 us
    dot_general x1, matrix products, attend(): jnp.einsum('hqk,khd->hqd', weights.astype(jnp.bfloat16), piece_values.res...  10.2 us
  transfers between devices with their start and end apart: 6, of which 4 were waited for; matrix products, arithmetic and copies ran while one was open for 6% of the time, Pallas kernels for 0%

commit v1 on v0

--- a/solution.py
+++ b/solution.py
@@ -11,6 +11,29 @@
 EPS = 1e-06
 THETA = 10000.0
 NEGATIVE = -1e30
+
+
+def in_blocks(shard, dim, devices):
+    dims = shard.shape
+    pieces = shard.reshape(*dims[:dim], devices, dims[dim] // devices, *dims[dim + 1 :])
+    return jnp.moveaxis(pieces, dim, 0)
+
+
+def laid_out(blocks, dim):
+    blocks = jnp.moveaxis(blocks, 0, dim)
+    lengths = blocks.shape
+    return blocks.reshape(*lengths[:dim], lengths[dim] * lengths[dim + 1], *lengths[dim + 2 :])
+
+
+def rotated_exchange(value, axis, split_dim, concat_dim):
+    size, here = (lax.axis_size(axis), lax.axis_index(axis))
+    blocks = in_blocks(value, split_dim, size)
+    outs = [blocks[here]]
+    for step in range(1, size):
+        sent = blocks[(here + step) % size]
+        outs.append(lax.ppermute(sent, axis, [(i, (i + step) % size) for i in range(size)]))
+    blocks = jnp.stack(outs)[(here - jnp.arange(size)) % size]
+    return laid_out(blocks, concat_dim)
 
 
 def copy_for_each(shard, axis):
@@ -207,7 +230,7 @@
     all_window, all_latent = in_one_piece((window_out, latent_out), "tp", 1, 0)
     column_window, column_latent = (
         lax.all_to_all(w_branch_window, "tp", split_axis=1, concat_axis=0, tiled=True),
-        lax.all_to_all(w_branch_latent, "tp", split_axis=1, concat_axis=0, tiled=True),
+        rotated_exchange(w_branch_latent, "tp", 1, 0),
     )
     window_branch = project(all_window, column_window)
     latent_branch = project(all_latent, column_latent)

time: 252 us -> 242 us (0.960)
  waiting for transfers between devices: 131 us -> 118 us
  starting transfers between devices: 15.8 us -> 20.5 us
    all_to_all x1 -> x0, waiting for transfers between devices: 10.4 us -> none  [on_device(): lax.all_to_all(w_branch_latent, 'tp', split_axis=1, concat_axis=0, tiled=...]
    all_to_all x1, waiting for transfers between devices: 9.8 us -> 0.01 us  [on_device(): lax.all_to_all(w_branch_window, 'tp', split_axis=1, concat_axis=0, tiled=...]
    ppermute x0 -> x7, starting transfers between devices: none -> 9.27 us  [rotated_exchange(): lax.ppermute(sent, axis, [(i, (i + step) % size) for i in range(size)])]
    ppermute x0 -> x7, waiting for transfers between devices: none -> 4.42 us  [rotated_exchange(): lax.ppermute(sent, axis, [(i, (i + step) % size) for i in range(size)])]
    all_to_all x1 -> x0, starting transfers between devices: 4.29 us -> none  [on_device(): lax.all_to_all(w_branch_latent, 'tp', split_axis=1, concat_axis=0, tiled=...]
    another operation x2 -> x12, local copies, waits for them, and re-layouts: 11.7 us -> 12.6 us
  transfers between devices with their start and end apart: 6 -> 12, of which waited for: 4 -> 7; matrix products, arithmetic and copies ran while one was open for 6% -> 31% of each run, Pallas kernels for 0% -> 0%
where the time goes in v1:
time: 242 us; the launch traced here: 240 us
  waiting for transfers between devices  118 us (49%)
  matrix products  52.3 us (22%)
  starting transfers between devices  20.5 us (8%)
  local copies, waits for them, and re-layouts  17.6 us (7%)
  other arithmetic  17.4 us (7%)
  between operations  14.3 us (6%)
    all_gather x2, waiting for transfers between devices, in_one_piece(): result = lax.all_gather(both, axis, axis=dim, tiled=True)  91.8 us
    all_to_all x1, waiting for transfers between devices, copy_for_each(): lax.all_to_all(jnp.broadcast_to(shard[None], (count, *shard.shape)), axis...  21.6 us
    dot_general x1, matrix products, attend(): jnp.einsum('qhr,kr->hqk', query_rotary, rope_piece, preferred_element_typ...  16.7 us
    dot_general x14, matrix products, project(): return jnp.dot(left, right, preferred_element_type=jnp.float32)  15 us
    another operation x11, local copies, waits for them, and re-layouts  12.6 us
    reduce_sum x1, other arithmetic, attend(): denominator = jnp.sum(weights, axis=-1)  11.1 us
    dot_general x1, matrix products, attend(): jnp.einsum('hqk,khd->hqd', weights.astype(jnp.bfloat16), piece_values.res...  10.2 us
    dot_general x1, matrix products, attend(): jnp.einsum('qhd,khd->hqk', query_content, piece_keys.reshape(piece_rows,...  9.75 us
  transfers between devices with their start and end apart: 12, of which 7 were waited for; matrix products, arithmetic and copies ran while one was open for 31% of the time, Pallas kernels for 0%

profile of v1, /device:TPU:36, one launch (start us, length us, event | category | flops | bytes accessed | tf_op | source)
XLA Modules:
  0.0 240.0 jit_solution(9318405399500083849)
XLA Ops:
  6.5 1.2 copy.42
  7.8 1.3 broadcast_in_dim.36
  9.1 4.5 %all-to-all-start = ((bf16[8,384,256]{1,2,0:T(8,128)(2,1)}), bf16[8,384,256]{1,2,0:T(8,128)(2,1)}, u32[]{:S(2)}, u32[]{:S(2)}) async-start(bf16[8,384,256]{1,2,0:T(8,128)(2,1)} %broadcast_in_dim.36), calls=%async_computation | async-start | bytes 3145728 | tf_op jit(solution)/shard_map/all_to_all | solution.py:41
  13.6 21.6 %all-to-all-done = bf16[8,384,256]{1,2,0:T(8,128)(2,1)} async-done(((bf16[8,384,256]{1,2,0:T(8,128)(2,1)}), bf16[8,384,256]{1,2,0:T(8,128)(2,1)}, u32[]{:S(2)}, u32[]{:S(2)}) %all-to-all-start) | async-done | bytes 1572896 | tf_op jit(solution)/shard_map/all_to_all | solution.py:41
  35.2 1.8 multiply_reduce_fusion
  37.0 1.8 fusion.19
  39.3 1.1 multiply_reduce_fusion.2
  41.5 0.7 pad_maximum_fusion
  42.3 1.0 copy.53
  43.3 3.5 %all-to-all-start.1 = ((bf16[128,8,256]{0,2,1:T(8,128)(2,1)}), bf16[128,8,256]{0,2,1:T(8,128)(2,1)S(1)}, u32[]{:S(2)}, u32[]{:S(2)}) async-start(bf16[128,8,256]{0,2,1:T(8,128)(2,1)} %bitcast.21), calls=%async_computation.1 | async-start | bytes 1048576 | tf_op jit(solution)/shard_map/all_to_all | solution.py:232
  47.9 1.3 convolution_convert_fusion.5
  49.3 3.2 %collective-permute-start = (bf16[128,128]{0,1:T(8,128)(2,1)S(1)}, bf16[128,128]{0,1:T(8,128)(2,1)S(1)}, u32[]{:S(2)}, u32[]{:S(2)}) collective-permute-start(bf16[128,128]{0,1:T(8,128)(2,1)S(1)} %pad_maximum_fusion.6), channel_id=1, source_target_pairs={{0,8},{8,16},{16,24},{24,32},{32,40},{40,48},{48,56},{56,64},{64,7... | collective-permute-start | bytes 98312 | tf_op jit(solution)/shard_map/ppermute | solution.py:60
  52.6 1.1 multiply_reduce_fusion.1
  56.7 86.6 %all-gather.3.cloned.1.call-done = bf16[12288,320]{0,1:T(8,128)(2,1)} async-done(((bf16[384,320]{0,1:T(8,128)(2,1)}), bf16[12288,320]{0,1:T(8,128)(2,1)}) %all-gather.3.cloned.1.call-update) | async-done | bytes 7864336 | tf_op jit(solution)/shard_map/all_gather | solution.py:66
  143.4 59.4 %conditional.1 = (f32[1,384]{1,0:T(1,128)S(1)}, f32[1,384,128]{1,2,0:T(8,128)S(1)}) conditional(s32[]{:T(128)} %convert_element_type.97, () %tuple.13, (s32[]{:T(128)}, s32[384]{0:T(512)S(1)}, bf16[12288,320]{0,1:T(8,128)(2,1)}, bf16[384,128]{1,0:T(8,128)(2,1)S(1)}, bf16[384,1,64]{0,2,1:T(8,128)(2,1)S(1)}) %tuple.14), branch_computations={%region_5.6_spmd, %region_6.9_spmd} | conditional | flops 3081240576 | bytes 119901712 | solution.py:222
  143.4 11.6 %copy.51 = bf16[12288,320]{1,0:T(8,128)(2,1)} copy(bf16[12288,320]{0,1:T(8,128)(2,1)} %get-tuple-element.44) | data formatting | bytes 15728640 | tf_op jit(solution)/shard_map
  155.0 9.7 %fusion.9 = f32[384,12288]{1,0:T(8,128)} fusion(bf16[384,128]{1,0:T(8,128)(2,1)S(1)} %get-tuple-element.25, bf16[12288,320]{1,0:T(8,128)(2,1)} %copy.51), kind=kOutput, calls=%fused_computation.12 | convolution fusion | flops 1207959552 | bytes 22118400 | tf_op jit(solution)/shard_map/cond/branch_1_fun/qhd,khd->hqk/dot_general | solution.py:190
  164.7 16.7 %fusion.65 = (f32[384]{0:T(512)S(1)}, f32[1,384,12288]{2,1,0:T(8,128)}) fusion(bf16[384,1,64]{0,2,1:T(8,128)(2,1)S(1)} %get-tuple-element.27, bf16[12288,320]{1,0:T(8,128)(2,1)} %copy.51, f32[384,12288]{1,0:T(8,128)} %fusion.9, s32[384]{0:T(512)S(1)} %broadcast_add_fusion), kind=kOutput, calls=%fused_computation.135 | convolution fusion | flops 627572352 | bytes 40946688 | tf_op jit(solution)/shard_map/cond/branch_1_fun/qhr,kr->hqk/dot_general | solution.py:196
  181.4 10.2 %fusion.11 = f32[1,384,128]{1,2,0:T(8,128)S(1)} fusion(bf16[12288,320]{1,0:T(8,128)(2,1)} %copy.51, f32[1,384,12288]{2,1,0:T(8,128)} %get-tuple-element.49, f32[384]{0:T(512)S(1)} %broadcast_maximum_fusion, s32[384]{0:T(512)S(1)} %broadcast_add_fusion), kind=kOutput, calls=%fused_computation.14 | convolution fusion | flops 1226833920 | bytes 22219776 | tf_op jit(solution)/shard_map/cond/branch_1_fun/hqk,khd->hqd/dot_general | solution.py:206
  191.7 11.1 %fusion.3 = f32[384]{0:T(512)S(1)} fusion(f32[1,384,12288]{2,1,0:T(8,128)} %get-tuple-element.49, f32[384]{0:T(512)S(1)} %broadcast_maximum_fusion, s32[384]{0:T(512)S(1)} %broadcast_add_fusion), kind=kLoop, calls=%fused_computation.7 | loop fusion | flops 18873984 | bytes 18878976 | tf_op jit(solution)/shard_map/cond/branch_1_fun/reduce_sum | solution.py:205
  203.8 1.6 collective-permute-start.2
  205.5 2.2 collective-permute-start.3
  207.8 2.3 collective-permute-start.4
  210.2 1.6 collective-permute-start.5
  212.3 1.5 collective-permute-start.6
  214.7 1.9 collective-permute-done.6
  216.6 1.7 collective-permute-done.7
  219.1 1.9 fusion.27
  221.1 3.0 %fusion.25 = f32[384,256]{1,0:T(8,128)} fusion(bf16[384,2048]{0,1:T(8,128)(2,1)} %copy-done.2, bf16[2048,256]{1,0:T(8,128)(2,1)S(1)} %copy-done.18), kind=kOutput, calls=%fused_computation.33 | convolution fusion | flops 402948096 | bytes 3014656 | tf_op jit(solution)/shard_map/dot_general | solution.py:97
  224.1 5.2 %all-gather.5.cloned.1.call-done = bf16[768,1024]{0,1:T(8,128)(2,1)} async-done(((bf16[768,128]{0,1:T(8,128)(2,1)}), bf16[768,1024]{0,1:T(8,128)(2,1)}) %all-gather.5.cloned.1.call-update) | async-done | bytes 1572880 | tf_op jit(solution)/shard_map/all_gather | solution.py:66
  229.3 1.6 convolution_multiply_fusion.2
  230.9 2.2 fusion.29
  (118 shorter events, 8.8 us)
Async XLA Ops:
  6.5 32.7 %copy-start = (bf16[2048,512]{1,0:T(8,128)(2,1)S(1)}, bf16[2048,512]{1,0:T(8,128)(2,1)}, u32[]{:S(2)}) copy-start(bf16[2048,512]{1,0:T(8,128)(2,1)} %param.28) | copy-start | bytes 6291460
  7.8 29.2 %copy-start.13 = (f32[2048]{0:T(1024)S(1)}, f32[2048]{0:T(1024)}, u32[]{:S(2)}) copy-start(f32[2048]{0:T(1024)} %param.22) | copy-start | bytes 24580
  9.1 26.1 %all-to-all-start = ((bf16[8,384,256]{1,2,0:T(8,128)(2,1)}), bf16[8,384,256]{1,2,0:T(8,128)(2,1)}, u32[]{:S(2)}, u32[]{:S(2)}) async-start(bf16[8,384,256]{1,2,0:T(8,128)(2,1)} %broadcast_in_dim.36), calls=%async_computation | async-start | bytes 3145728 | tf_op jit(solution)/shard_map/all_to_all | solution.py:41
  13.5 25.3 %copy-start.8 = (bf16[2048,64]{0,1:T(8,128)(2,1)S(1)}, bf16[2048,64]{0,1:T(8,128)(2,1)}, u32[]{:S(2)}) copy-start(bf16[2048,64]{0,1:T(8,128)(2,1)} %param.29) | copy-start | bytes 786436
  13.5 129.8 %all-gather.3.cloned.1.call-start = ((), (), s32[]{:S(2)}) async-start(), calls=%async_computation.2 | async-start | bytes 8110080 | tf_op jit(solution)/shard_map/all_gather | solution.py:66
  38.9 1.5 copy-start.2
  39.3 1.2 copy-start.9
  39.3 1.2 copy-start.14
  39.3 1.6 copy-start.10
  39.3 3.0 %copy-start.4 = (bf16[128,2048]{1,0:T(8,128)(2,1)S(1)}, bf16[128,2048]{1,0:T(8,128)(2,1)}, u32[]{:S(2)}) copy-start(bf16[128,2048]{1,0:T(8,128)(2,1)} %param.36) | copy-start | bytes 1572868
  40.4 6.5 %copy-start.5 = (bf16[128,2048]{1,0:T(8,128)(2,1)S(1)}, bf16[128,2048]{1,0:T(8,128)(2,1)}, u32[]{:S(2)}) copy-start(bf16[128,2048]{1,0:T(8,128)(2,1)} %param.37) | copy-start | bytes 1572868
  40.4 7.1 %copy-start.3 = (bf16[384,2048]{0,1:T(8,128)(2,1)S(1)}, bf16[384,2048]{0,1:T(8,128)(2,1)}, u32[]{:S(2)}) copy-start(bf16[384,2048]{0,1:T(8,128)(2,1)} %copy-done.2) | copy-start | bytes 4718596
  40.5 7.1 %copy-start.7 = (bf16[2048,64]{0,1:T(8,128)(2,1)S(1)}, bf16[2048,64]{0,1:T(8,128)(2,1)}, u32[]{:S(2)}) copy-start(bf16[2048,64]{0,1:T(8,128)(2,1)} %param.24) | copy-start | bytes 786436
  43.3 175.6 %all-to-all-start.1 = ((bf16[128,8,256]{0,2,1:T(8,128)(2,1)}), bf16[128,8,256]{0,2,1:T(8,128)(2,1)S(1)}, u32[]{:S(2)}, u32[]{:S(2)}) async-start(bf16[128,8,256]{0,2,1:T(8,128)(2,1)} %bitcast.21), calls=%async_computation.1 | async-start | bytes 1048576 | tf_op jit(solution)/shard_map/all_to_all | solution.py:232
  46.8 182.5 %all-gather.5.cloned.1.call-start = ((), (), s32[]{:S(2)}) async-start(), calls=%async_computation.3 | async-start | bytes 1769472 | tf_op jit(solution)/shard_map/all_gather | solution.py:66
  47.2 5.3 %copy-start.17 = (bf16[2048,512]{1,0:T(8,128)(2,1)S(1)}, bf16[2048,512]{1,0:T(8,128)(2,1)}, u32[]{:S(2)}) copy-start(bf16[2048,512]{1,0:T(8,128)(2,1)} %param.27) | copy-start | bytes 6291460
  49.3 4.4 %copy-start.12 = (bf16[512,64]{0,1:T(8,128)(2,1)S(1)}, bf16[512,64]{0,1:T(8,128)(2,1)}, u32[]{:S(2)}) copy-start(bf16[512,64]{0,1:T(8,128)(2,1)} %param.33) | copy-start | bytes 196612
  49.3 4.4 %copy-start.15 = (f32[512]{0:T(512)S(1)}, f32[512]{0:T(512)}, u32[]{:S(2)}) copy-start(f32[512]{0:T(512)} %param.30) | copy-start | bytes 6148
  49.3 5.0 %copy-start.11 = (bf16[512,128]{1,0:T(8,128)(2,1)S(1)}, bf16[512,128]{1,0:T(8,128)(2,1)}, u32[]{:S(2)}) copy-start(bf16[512,128]{1,0:T(8,128)(2,1)} %param.32) | copy-start | bytes 393220
  49.3 5.4 %copy-start.6 = (bf16[2048,128]{1,0:T(8,128)(2,1)S(1)}, bf16[2048,128]{1,0:T(8,128)(2,1)}, u32[]{:S(2)}) copy-start(bf16[2048,128]{1,0:T(8,128)(2,1)} %param.23) | copy-start | bytes 1572868
  49.3 6.2 %collective-permute-start = (bf16[128,128]{0,1:T(8,128)(2,1)S(1)}, bf16[128,128]{0,1:T(8,128)(2,1)S(1)}, u32[]{:S(2)}, u32[]{:S(2)}) collective-permute-start(bf16[128,128]{0,1:T(8,128)(2,1)S(1)} %pad_maximum_fusion.6), channel_id=1, source_target_pairs={{0,8},{8,16},{16,24},{24,32},{32,40},{40,48},{48,56},{56,64},{64,7... | collective-permute-start | bytes 98312 | tf_op jit(solution)/shard_map/ppermute | solution.py:60
  54.3 1.6 copy-start.16
  203.7 8.6 %collective-permute-start.1 = (bf16[128,256]{1,0:T(8,128)(2,1)S(1)}, bf16[128,256]{1,0:T(8,128)(2,1)S(1)}, u32[]{:S(2)}, u32[]{:S(2)}) collective-permute-start(bf16[128,256]{1,0:T(8,128)(2,1)S(1)} %bitcast.142), channel_id=1, source_target_pairs={{0,1},{1,2},{2,3},{3,4},{4,5},{5,6},{6,7},{7,0},{8,9},{9,10},{10,1... | collective-permute-start | bytes 196616 | tf_op jit(solution)/shard_map/ppermute | solution.py:34
  203.8 10.0 %collective-permute-start.2 = (bf16[128,256]{1,0:T(8,128)(2,1)S(1)}, bf16[128,256]{1,0:T(8,128)(2,1)S(1)}, u32[]{:S(2)}, u32[]{:S(2)}) collective-permute-start(bf16[128,256]{1,0:T(8,128)(2,1)S(1)} %bitcast.141), channel_id=1, source_target_pairs={{0,2},{1,3},{2,4},{3,5},{4,6},{5,7},{6,0},{7,1},{8,10},{9,11},{10,... | collective-permute-start | bytes 196616 | tf_op jit(solution)/shard_map/ppermute | solution.py:34
  205.5 8.3 %collective-permute-start.3 = (bf16[128,256]{1,0:T(8,128)(2,1)S(1)}, bf16[128,256]{1,0:T(8,128)(2,1)S(1)}, u32[]{:S(2)}, u32[]{:S(2)}) collective-permute-start(bf16[128,256]{1,0:T(8,128)(2,1)S(1)} %bitcast.140), channel_id=1, source_target_pairs={{0,3},{1,4},{2,5},{3,6},{4,7},{5,0},{6,1},{7,2},{8,11},{9,12},{10,... | collective-permute-start | bytes 196616 | tf_op jit(solution)/shard_map/ppermute | solution.py:34
  207.8 6.5 %collective-permute-start.4 = (bf16[128,256]{1,0:T(8,128)(2,1)S(1)}, bf16[128,256]{1,0:T(8,128)(2,1)S(1)}, u32[]{:S(2)}, u32[]{:S(2)}) collective-permute-start(bf16[128,256]{1,0:T(8,128)(2,1)S(1)} %bitcast.138), channel_id=1, source_target_pairs={{0,4},{1,5},{2,6},{3,7},{4,0},{5,1},{6,2},{7,3},{8,12},{9,13},{10,... | collective-permute-start | bytes 196616 | tf_op jit(solution)/shard_map/ppermute | solution.py:34
  210.2 4.5 %collective-permute-start.5 = (bf16[128,256]{1,0:T(8,128)(2,1)S(1)}, bf16[128,256]{1,0:T(8,128)(2,1)S(1)}, u32[]{:S(2)}, u32[]{:S(2)}) collective-permute-start(bf16[128,256]{1,0:T(8,128)(2,1)S(1)} %bitcast.137), channel_id=1, source_target_pairs={{0,5},{1,6},{2,7},{3,0},{4,1},{5,2},{6,3},{7,4},{8,13},{9,14},{10,... | collective-permute-start | bytes 196616 | tf_op jit(solution)/shard_map/ppermute | solution.py:34
  212.3 4.3 %collective-permute-start.6 = (bf16[128,256]{1,0:T(8,128)(2,1)S(1)}, bf16[128,256]{1,0:T(8,128)(2,1)S(1)}, u32[]{:S(2)}, u32[]{:S(2)}) collective-permute-start(bf16[128,256]{1,0:T(8,128)(2,1)S(1)} %bitcast.139), channel_id=1, source_target_pairs={{0,6},{1,7},{2,0},{3,1},{4,2},{5,3},{6,4},{7,5},{8,14},{9,15},{10,... | collective-permute-start | bytes 196616 | tf_op jit(solution)/shard_map/ppermute | solution.py:34
  213.8 4.5 %collective-permute-start.7 = (bf16[128,256]{1,0:T(8,128)(2,1)S(1)}, bf16[128,256]{1,0:T(8,128)(2,1)S(1)}, u32[]{:S(2)}, u32[]{:S(2)}) collective-permute-start(bf16[128,256]{1,0:T(8,128)(2,1)S(1)} %bitcast.136), channel_id=1, source_target_pairs={{0,7},{1,0},{2,1},{3,2},{4,3},{5,4},{6,5},{7,6},{8,15},{9,8},{10,9... | collective-permute-start | bytes 196616 | tf_op jit(solution)/shard_map/ppermute | solution.py:34
  219.1 2.0 copy-start.18
  221.1 12.0 %copy-start.1 = (bf16[2048,512]{1,0:T(8,128)(2,1)S(1)}, bf16[2048,512]{1,0:T(8,128)(2,1)}, u32[]{:S(2)}) copy-start(bf16[2048,512]{1,0:T(8,128)(2,1)} %param.28) | copy-start | bytes 6291460
Sparse Core Ops, SparseCore 0:
  42.4 100.9 all-gather.2
  203.6 25.5 all-gather.4
